TPU v7x, 128 devices: a whole 4x4x4 slice. The times are simulated.
128 devices in a mesh: fs: 16 (over z, x), tp: 8 (over y, core).
Axes of the slice: x: 4, y: 4, z: 4, core: 2. Of those that a mesh axis runs over, the one named last changes fastest.
Arguments:
- tokens: bfloat16 [32, 384, 2048], P('fs', None, 'tp'), may hold values from -20 to 20
- first_gain: float32 [2048], replicated, may hold values from 0.1 to 1.9
- first_gate: bfloat16 [2048, 5120], P('fs', 'tp'), may hold values from -0.125 to 0.125
- first_up: bfloat16 [2048, 5120], P('fs', 'tp'), may hold values from -0.125 to 0.125
- first_down: bfloat16 [5120, 2048], P('tp', 'fs'), may hold values from -0.078125 to 0.078125
- mixer_gain: float32 [2048], replicated, may hold values from 0.1 to 1.9
- conv_input: bfloat16 [2048, 1024], P('fs', 'tp'), may hold values from -0.125 to 0.125
- outer_gate: bfloat16 [2048, 1024], P('fs', 'tp'), may hold values from -0.125 to 0.125
- inner_gate: bfloat16 [2048, 1024], P('fs', 'tp'), may hold values from -0.125 to 0.125
- conv_taps: float32 [3, 1024], P(None, 'tp'), may hold values from -3.5 to 3.5
- mixer_out: bfloat16 [1024, 2048], P('tp', 'fs'), may hold values from -0.1875 to 0.1875
- second_gain: float32 [2048], replicated, may hold values from 0.1 to 1.9
- second_gate: bfloat16 [2048, 5120], P('fs', 'tp'), may hold values from -0.125 to 0.125
- second_up: bfloat16 [2048, 5120], P('fs', 'tp'), may hold values from -0.125 to 0.125
- second_down: bfloat16 [5120, 2048], P('tp', 'fs'), may hold values from -0.078125 to 0.078125
Outputs:
- layer_out: bfloat16 [32, 384, 2048], P('fs', None, 'tp')
All inputs are finite; a program needn't handle non-finite values.
Results may differ from a plain program's by a relative error of at most 0.015.
Values may be sent and summed in bfloat16 or wider, within the bound.
A program may use at most 64 MiB of HBM per device.

v0:
```python
import jax
import jax.numpy as jnp
from jax import lax
from jax.sharding import PartitionSpec as P

epsilon = 1e-05


def sent_together(arrays, axis, dim, along):
    ends, at = ([], 0)
    for a in arrays[:-1]:
        at += a.shape[along]
        ends.append(at)
    both = jnp.concatenate(arrays, axis=along)
    return tuple(jnp.split(lax.all_gather(both, axis, axis=dim, tiled=True), ends, axis=along))


def copy_for_each(value, axis):
    copies = jnp.broadcast_to(value, (lax.axis_size(axis), *value.shape))
    return lax.all_to_all(copies, axis, split_axis=0, concat_axis=0, tiled=True)


def joined_along(pieces, dim):
    shape = list(pieces.shape[1:])
    shape[dim] *= pieces.shape[0]
    return jnp.moveaxis(pieces, 0, dim).reshape(shape)


def gathered_copies(value, axis, dim):
    pieces = copy_for_each(value, axis)
    return joined_along(pieces, dim)


def norm_rows(stream, gain):
    whole = lax.all_gather(stream, "tp", axis=1, tiled=True)
    values = whole.astype(jnp.float32)
    scale = lax.rsqrt(jnp.mean(values * values, axis=1, keepdims=True) + epsilon)
    return (values * scale * gain).astype(jnp.bfloat16)


def add_rows(gathered, piece):
    return jnp.dot(gathered, piece, preferred_element_type=jnp.float32)


def ffn_inputs(gathered, gate_weight, up_weight):
    pieces = sent_together((gate_weight, up_weight), "fs", 0, 1)
    gate = add_rows(gathered, pieces[0])
    upward = add_rows(gathered, pieces[1])
    return (gate, upward)


def mixer_inputs(gathered, conv_input, outer_gate, inner_gate):
    pieces = sent_together((conv_input, outer_gate, inner_gate), "fs", 0, 1)
    conv_values = add_rows(gathered, pieces[0])
    outer = add_rows(gathered, pieces[1])
    inner = add_rows(gathered, pieces[2])
    return (conv_values, outer, inner)


def project_down(hidden, weight):
    partial_sum = jnp.dot(
        hidden, gathered_copies(weight, "fs", 1), preferred_element_type=jnp.float32
    )
    result = lax.psum_scatter(
        partial_sum.astype(jnp.bfloat16), "tp", scatter_dimension=1, tiled=True
    ).astype(jnp.float32)
    return result


def half_ffn(stream, gain, gate_weight, up_weight, down_weight):
    gathered = norm_rows(stream, gain)
    gate, upward = ffn_inputs(gathered, gate_weight, up_weight)
    hidden = (jax.nn.silu(gate) * upward).astype(jnp.bfloat16)
    branch = project_down(hidden, down_weight)
    return (stream.astype(jnp.float32) + 0.5 * branch).astype(jnp.bfloat16)


def conv_mixer(stream, seqs, gain, conv_input, outer_gate, inner_gate, conv_taps, mixer_out):
    gathered = norm_rows(stream, gain)
    conv_values, outer, inner = mixer_inputs(gathered, conv_input, outer_gate, inner_gate)
    gated_input = (inner * conv_values).reshape(seqs, -1, conv_values.shape[1])
    one_back = jnp.pad(gated_input, ((0, 0), (1, 0), (0, 0)))[:, :-1]
    two_back = jnp.pad(gated_input, ((0, 0), (2, 0), (0, 0)))[:, :-2]
    convolved = conv_taps[0] * two_back + conv_taps[1] * one_back + conv_taps[2] * gated_input
    mixed = (outer * convolved.reshape(conv_values.shape)).astype(jnp.bfloat16)
    branch = project_down(mixed, mixer_out)
    return (stream.astype(jnp.float32) + branch).astype(jnp.bfloat16)


def on_device(
    tokens,
    first_gain,
    first_gate,
    first_up,
    first_down,
    mixer_gain,
    conv_input,
    outer_gate,
    inner_gate,
    conv_taps,
    mixer_out,
    second_gain,
    second_gate,
    second_up,
    second_down,
):
    seqs, length, width = tokens.shape
    stream = tokens.reshape(seqs * length, width)
    stream = half_ffn(stream, first_gain, first_gate, first_up, first_down)
    stream = conv_mixer(
        stream, seqs, mixer_gain, conv_input, outer_gate, inner_gate, conv_taps, mixer_out
    )
    stream = half_ffn(stream, second_gain, second_gate, second_up, second_down)
    return stream.reshape(seqs, length, width)


def solution(mesh):
    in_specs = (
        P("fs", None, "tp"),
        P(),
        P("fs", "tp"),
        P("fs", "tp"),
        P("tp", "fs"),
        P(),
        P("fs", "tp"),
        P("fs", "tp"),
        P("fs", "tp"),
        P(None, "tp"),
        P("tp", "fs"),
        P(),
        P("fs", "tp"),
        P("fs", "tp"),
        P("tp", "fs"),
    )
    out_specs = P("fs", None, "tp")
    return jax.shard_map(
        on_device, mesh=mesh, in_specs=in_specs, out_specs=out_specs, check_vma=False
    )
```

profile of v0, /device:TPU:0, one launch (start us, length us, event | category | flops | bytes accessed | tf_op | source)
XLA Modules:
  0.0 431.1 jit_solution(13457404551450091952)
XLA Ops:
  10.1 1.9 broadcast_in_dim.6
  12.0 8.2 %all-to-all-start = ((bf16[16,640,128]{1,2,0:T(8,128)(2,1)}), bf16[16,640,128]{1,2,0:T(8,128)(2,1)}, u32[]{:S(2)}, u32[]{:S(2)}) async-start(bf16[16,640,128]{1,2,0:T(8,128)(2,1)} %broadcast_in_dim.6), calls=%async_computation | async-start | bytes 5242880 | tf_op jit(solution)/shard_map/all_to_all | solution.py:20
  20.3 22.4 %all-gather.7.cloned.1.call-done = bf16[768,2048]{1,0:T(8,128)(2,1)} async-done(((bf16[768,256]{1,0:T(8,128)(2,1)}), bf16[768,2048]{1,0:T(8,128)(2,1)}) %all-gather.7.cloned.1.call-update) | async-done | bytes 3145744 | tf_op jit(solution)/shard_map/all_gather | solution.py:35
  42.7 2.7 fusion
  45.4 56.7 %all-gather.9.cloned.1.call-done = bf16[2048,1280]{1,0:T(8,128)(2,1)} async-done(((bf16[128,1280]{1,0:T(8,128)(2,1)}), bf16[2048,1280]{1,0:T(8,128)(2,1)}) %all-gather.9.cloned.1.call-update) | async-done | bytes 5242896 | tf_op jit(solution)/shard_map/all_gather | solution.py:15
  102.1 5.7 %fusion.15 = f32[768,640]{1,0:T(8,128)} fusion(bf16[2048,1280]{1,0:T(8,128)(2,1)} %all-gather.9.cloned.1.call-done, bf16[768,2048]{1,0:T(8,128)(2,1)S(1)} %copy-done.3, f32[2048]{0:T(1024)S(1)} %copy-done.15, f32[768]{0:T(1024)S(1)} %add_rsqrt_fusion.2), kind=kOutput, calls=%fused_computation.24 | convolution fusion | flops 2019557376 | bytes 7744512 | tf_op jit(solution)/shard_map/dot_general | solution.py:42
  107.8 10.7 %convolution_convert_fusion.1 = bf16[768,2048]{1,0:T(8,128)(2,1)} fusion(bf16[640,2048]{0,1:T(8,128)(2,1)} %bitcast.2, f32[768,640]{1,0:T(8,128)} %fusion.15, bf16[2048,1280]{1,0:T(8,128)(2,1)} %all-gather.9.cloned.1.call-done, bf16[768,2048]{1,0:T(8,128)(2,1)S(1)} %copy-done.3, f32[2048]{0:T(1024)S(1)} %copy-done.15, f32[768]{0:T(1024)S(1)} %add_rsqrt_fusion.2), kind=kOutput, calls=%fused_computation.16 | convolution fusion | flops 4037345280 | bytes 13511680 | tf_op jit(solution)/shard_map/dot_general | solution.py:61
  118.6 35.6 %reduce-scatter.4.cloned.1.call-done = bf16[768,256]{1,0:T(8,128)(2,1)} async-done(((bf16[768,2048]{1,0:T(8,128)(2,1)}), bf16[768,256]{1,0:T(8,128)(2,1)}) %reduce-scatter.4.cloned.1.call-update) | async-done | bytes 393232 | tf_op jit(solution)/shard_map/reduce_scatter | solution.py:64
  157.9 7.0 %all-to-all-start.1 = ((bf16[16,128,128]{1,2,0:T(8,128)(2,1)}), bf16[16,128,128]{1,2,0:T(8,128)(2,1)}, u32[]{:S(2)}, u32[]{:S(2)}) async-start(bf16[16,128,128]{1,2,0:T(8,128)(2,1)} %broadcast_in_dim.7), calls=%async_computation.2 | async-start | bytes 1048576 | tf_op jit(solution)/shard_map/all_to_all | solution.py:20
  165.2 21.0 %all-gather.11.cloned.1.call-done = bf16[768,2048]{1,0:T(8,128)(2,1)} async-done(((bf16[768,256]{1,0:T(8,128)(2,1)}), bf16[768,2048]{1,0:T(8,128)(2,1)}) %all-gather.11.cloned.1.call-update) | async-done | bytes 3145744 | tf_op jit(solution)/shard_map/all_gather | solution.py:35
  186.2 2.7 fusion.3
  189.8 43.1 %all-gather.13.cloned.1.call-done = bf16[2048,384]{1,0:T(8,128)(2,1)} async-done(((bf16[128,384]{1,0:T(8,128)(2,1)}), bf16[2048,384]{1,0:T(8,128)(2,1)}) %all-gather.13.cloned.1.call-update) | async-done | bytes 1572880 | tf_op jit(solution)/shard_map/all_gather | solution.py:15
  233.0 2.0 fusion.35
  235.0 2.0 convolution_multiply_fusion
  237.1 6.2 %convolution_convert_fusion.2 = bf16[768,2048]{1,0:T(8,128)(2,1)} fusion(bf16[128,2048]{0,1:T(8,128)(2,1)} %bitcast.9, f32[768,128]{1,0:T(8,128)S(1)} %bitcast.28, bf16[768,2048]{1,0:T(8,128)(2,1)S(1)} %fusion.5, bf16[2048,384]{1,0:T(8,128)(2,1)} %all-gather.13.cloned.1.call-done), kind=kOutput, calls=%fused_computation.17 | convolution fusion | flops 807075840 | bytes 7733248 | tf_op jit(solution)/shard_map/dot_general | solution.py:61
  243.4 35.3 %reduce-scatter.6.cloned.1.call-done = bf16[768,256]{1,0:T(8,128)(2,1)} async-done(((bf16[768,2048]{1,0:T(8,128)(2,1)}), bf16[768,256]{1,0:T(8,128)(2,1)}) %reduce-scatter.6.cloned.1.call-update) | async-done | bytes 393232 | tf_op jit(solution)/shard_map/reduce_scatter | solution.py:64
  281.6 1.9 broadcast_in_dim.8
  283.5 7.1 %all-to-all-start.2 = ((bf16[16,640,128]{1,2,0:T(8,128)(2,1)}), bf16[16,640,128]{1,2,0:T(8,128)(2,1)}, u32[]{:S(2)}, u32[]{:S(2)}) async-start(bf16[16,640,128]{1,2,0:T(8,128)(2,1)} %broadcast_in_dim.8), calls=%async_computation.4 | async-start | bytes 5242880 | tf_op jit(solution)/shard_map/all_to_all | solution.py:20
  290.9 19.8 %all-gather.15.cloned.1.call-done = bf16[768,2048]{1,0:T(8,128)(2,1)} async-done(((bf16[768,256]{1,0:T(8,128)(2,1)}), bf16[768,2048]{1,0:T(8,128)(2,1)}) %all-gather.15.cloned.1.call-update) | async-done | bytes 3145744 | tf_op jit(solution)/shard_map/all_gather | solution.py:35
  310.7 2.7 fusion.6
  313.4 57.2 %all-gather.17.cloned.1.call-done = bf16[2048,1280]{1,0:T(8,128)(2,1)} async-done(((bf16[128,1280]{1,0:T(8,128)(2,1)}), bf16[2048,1280]{1,0:T(8,128)(2,1)}) %all-gather.17.cloned.1.call-update) | async-done | bytes 5242896 | tf_op jit(solution)/shard_map/all_gather | solution.py:15
  370.6 5.7 %fusion.11 = f32[768,640]{1,0:T(8,128)} fusion(bf16[2048,1280]{1,0:T(8,128)(2,1)} %all-gather.17.cloned.1.call-done, bf16[768,2048]{1,0:T(8,128)(2,1)S(1)} %copy-done.4, f32[2048]{0:T(1024)S(1)} %copy-done.16, f32[768]{0:T(1024)S(1)} %add_rsqrt_fusion), kind=kOutput, calls=%fused_computation.20 | convolution fusion | flops 2019557376 | bytes 7744512 | tf_op jit(solution)/shard_map/dot_general | solution.py:42
  376.3 10.7 %convolution_convert_fusion = bf16[768,2048]{1,0:T(8,128)(2,1)} fusion(bf16[640,2048]{0,1:T(8,128)(2,1)} %bitcast.11, f32[768,640]{1,0:T(8,128)} %fusion.11, bf16[2048,1280]{1,0:T(8,128)(2,1)} %all-gather.17.cloned.1.call-done, bf16[768,2048]{1,0:T(8,128)(2,1)S(1)} %copy-done.4, f32[2048]{0:T(1024)S(1)} %copy-done.16, f32[768]{0:T(1024)S(1)} %add_rsqrt_fusion), kind=kOutput, calls=%fused_computation.15 | convolution fusion | flops 4037345280 | bytes 13511680 | tf_op jit(solution)/shard_map/dot_general | solution.py:61
  387.0 35.7 %reduce-scatter.8.cloned.1.call-done = bf16[768,256]{1,0:T(8,128)(2,1)} async-done(((bf16[768,2048]{1,0:T(8,128)(2,1)}), bf16[768,256]{1,0:T(8,128)(2,1)}) %reduce-scatter.8.cloned.1.call-update) | async-done | bytes 393232 | tf_op jit(solution)/shard_map/reduce_scatter | solution.py:64
  (71 shorter events, 13.6 us)
Async XLA Ops:
  6.5 36.1 %all-gather.7.cloned.1.call-start = ((), (), s32[]{:S(2)}) async-start(), calls=%async_computation.6 | async-start | bytes 3538944 | tf_op jit(solution)/shard_map/all_gather | solution.py:35
  7.3 94.8 %all-gather.9.cloned.1.call-start = ((), (), s32[]{:S(2)}) async-start(), calls=%async_computation.7 | async-start | bytes 5570560 | tf_op jit(solution)/shard_map/all_gather | solution.py:15
  12.0 90.1 %copy-start.15 = (f32[2048]{0:T(1024)S(1)}, f32[2048]{0:T(1024)}, u32[]{:S(2)}) copy-start(f32[2048]{0:T(1024)} %param.16) | copy-start | bytes 24580
  12.0 95.8 %all-to-all-start = ((bf16[16,640,128]{1,2,0:T(8,128)(2,1)}), bf16[16,640,128]{1,2,0:T(8,128)(2,1)}, u32[]{:S(2)}, u32[]{:S(2)}) async-start(bf16[16,640,128]{1,2,0:T(8,128)(2,1)} %broadcast_in_dim.6), calls=%async_computation | async-start | bytes 5242880 | tf_op jit(solution)/shard_map/all_to_all | solution.py:20
  20.2 134.0 %reduce-scatter.4.cloned.1.call-start = ((), (), s32[]{:S(2)}) async-start(), calls=%async_computation.8 | async-start | bytes 3538944 | tf_op jit(solution)/shard_map/reduce_scatter | solution.py:64
  42.7 59.5 %copy-start.3 = (bf16[768,2048]{1,0:T(8,128)(2,1)S(1)}, bf16[768,2048]{1,0:T(8,128)(2,1)}, u32[]{:S(2)}) copy-start(bf16[768,2048]{1,0:T(8,128)(2,1)} %all-gather.7.cloned.1.call-done) | copy-start | bytes 9437188
  118.5 37.7 %copy-start.10 = (bf16[128,128]{1,0:T(8,128)(2,1)S(1)}, bf16[128,128]{1,0:T(8,128)(2,1)}, u32[]{:S(2)}) copy-start(bf16[128,128]{1,0:T(8,128)(2,1)} %param.23) | copy-start | bytes 98308
  118.5 37.7 %copy-start.11 = (bf16[128,128]{1,0:T(8,128)(2,1)S(1)}, bf16[128,128]{1,0:T(8,128)(2,1)}, u32[]{:S(2)}) copy-start(bf16[128,128]{1,0:T(8,128)(2,1)} %param.22) | copy-start | bytes 98308
  118.5 37.7 %copy-start.12 = (bf16[128,128]{1,0:T(8,128)(2,1)S(1)}, bf16[128,128]{1,0:T(8,128)(2,1)}, u32[]{:S(2)}) copy-start(bf16[128,128]{1,0:T(8,128)(2,1)} %param.21) | copy-start | bytes 98308
  118.5 38.3 %copy-start.9 = (bf16[128,128]{1,0:T(8,128)(2,1)S(1)}, bf16[128,128]{1,0:T(8,128)(2,1)}, u32[]{:S(2)}) copy-start(bf16[128,128]{1,0:T(8,128)(2,1)} %param.25) | copy-start | bytes 98308
  118.5 46.6 %copy-start.14 = (f32[3,128]{1,0:T(4,128)S(1)}, f32[3,128]{1,0:T(4,128)}, u32[]{:S(2)}) copy-start(f32[3,128]{1,0:T(4,128)} %param.24) | copy-start | bytes 4612
  118.5 70.4 %copy-start.13 = (f32[2048]{0:T(1024)S(1)}, f32[2048]{0:T(1024)}, u32[]{:S(2)}) copy-start(f32[2048]{0:T(1024)} %param.20) | copy-start | bytes 24580
  118.6 67.6 %all-gather.11.cloned.1.call-start = ((), (), s32[]{:S(2)}) async-start(), calls=%async_computation.9 | async-start | bytes 3538944 | tf_op jit(solution)/shard_map/all_gather | solution.py:35
  156.1 76.9 %all-gather.13.cloned.1.call-start = ((), (), s32[]{:S(2)}) async-start(), calls=%async_computation.10 | async-start | bytes 1671168 | tf_op jit(solution)/shard_map/all_gather | solution.py:15
  157.9 79.2 %all-to-all-start.1 = ((bf16[16,128,128]{1,2,0:T(8,128)(2,1)}), bf16[16,128,128]{1,2,0:T(8,128)(2,1)}, u32[]{:S(2)}, u32[]{:S(2)}) async-start(bf16[16,128,128]{1,2,0:T(8,128)(2,1)} %broadcast_in_dim.7), calls=%async_computation.2 | async-start | bytes 1048576 | tf_op jit(solution)/shard_map/all_to_all | solution.py:20
  164.9 113.8 %reduce-scatter.6.cloned.1.call-start = ((), (), s32[]{:S(2)}) async-start(), calls=%async_computation.11 | async-start | bytes 3538944 | tf_op jit(solution)/shard_map/reduce_scatter | solution.py:64
  243.3 37.3 %copy-start.7 = (bf16[128,640]{1,0:T(8,128)(2,1)S(1)}, bf16[128,640]{1,0:T(8,128)(2,1)}, u32[]{:S(2)}) copy-start(bf16[128,640]{1,0:T(8,128)(2,1)} %param.27) | copy-start | bytes 491524
  243.3 38.1 %copy-start.8 = (bf16[640,128]{1,0:T(8,128)(2,1)S(1)}, bf16[640,128]{1,0:T(8,128)(2,1)}, u32[]{:S(2)}) copy-start(bf16[640,128]{1,0:T(8,128)(2,1)} %param.29) | copy-start | bytes 491524
  243.3 67.3 %all-gather.15.cloned.1.call-start = ((), (), s32[]{:S(2)}) async-start(), calls=%async_computation.12 | async-start | bytes 3538944 | tf_op jit(solution)/shard_map/all_gather | solution.py:35
  280.6 90.0 %all-gather.17.cloned.1.call-start = ((), (), s32[]{:S(2)}) async-start(), calls=%async_computation.13 | async-start | bytes 5570560 | tf_op jit(solution)/shard_map/all_gather | solution.py:15
  283.5 87.1 %copy-start.16 = (f32[2048]{0:T(1024)S(1)}, f32[2048]{0:T(1024)}, u32[]{:S(2)}) copy-start(f32[2048]{0:T(1024)} %param.26) | copy-start | bytes 24580
  283.5 92.8 %all-to-all-start.2 = ((bf16[16,640,128]{1,2,0:T(8,128)(2,1)}), bf16[16,640,128]{1,2,0:T(8,128)(2,1)}, u32[]{:S(2)}, u32[]{:S(2)}) async-start(bf16[16,640,128]{1,2,0:T(8,128)(2,1)} %broadcast_in_dim.8), calls=%async_computation.4 | async-start | bytes 5242880 | tf_op jit(solution)/shard_map/all_to_all | solution.py:20
  290.6 132.1 %reduce-scatter.8.cloned.1.call-start = ((), (), s32[]{:S(2)}) async-start(), calls=%async_computation.14 | async-start | bytes 3538944 | tf_op jit(solution)/shard_map/reduce_scatter | solution.py:64
  310.7 60.0 %copy-start.4 = (bf16[768,2048]{1,0:T(8,128)(2,1)S(1)}, bf16[768,2048]{1,0:T(8,128)(2,1)}, u32[]{:S(2)}) copy-start(bf16[768,2048]{1,0:T(8,128)(2,1)} %all-gather.15.cloned.1.call-done) | copy-start | bytes 9437188
  (5 other events, 147.0 us)
Sparse Core Ops, SparseCore 0:
  9.0 33.5 all-gather.6
  44.8 57.2 all-gather.8
  118.7 35.4 reduce-scatter.3
  156.2 29.9 all-gather.10
  188.2 44.7 all-gather.12
  243.5 35.2 reduce-scatter.5
  280.7 29.9 all-gather.14
  312.8 57.7 all-gather.16
  387.1 35.4 reduce-scatter.7
where the time goes:
time: 432 us; the launch traced here: 431 us
  waiting for transfers between devices  328 us (76%)
  matrix products  42.9 us (10%)
  starting transfers between devices  23 us (5%)
  other arithmetic  17.8 us (4%)
  between operations  13.4 us (3%)
  local copies, waits for them, and re-layouts  6.23 us (1%)
    all_gather x3, waiting for transfers between devices, sent_together(): lax.all_gather(both, axis, axis=dim, tiled=True)  157 us
    reduce_scatter x3, waiting for transfers between devices, project_down(): lax.psum_scatter(partial_sum.astype(jnp.bfloat16), 'tp', scatter_dimensio...  107 us
    all_gather x3, waiting for transfers between devices, norm_rows(): whole = lax.all_gather(stream, 'tp', axis=1, tiled=True)  63.2 us
    dot_general x3, matrix products, project_down(): jnp.dot(hidden, gathered_copies(weight, 'fs', 1), preferred_element_type=...  27.5 us
    all_to_all x3, starting transfers between devices, copy_for_each(): return lax.all_to_all(copies, axis, split_axis=0, concat_axis=0, tiled=True)  22.3 us
    dot_general x4, matrix products, add_rows(): return jnp.dot(gathered, piece, preferred_element_type=jnp.float32)  15.4 us
  transfers between devices with their start and end apart: 12, of which 9 were waited for; matrix products, arithmetic and copies ran while one was open for 8% of the time, Pallas kernels for 0%

commit v1 on v0

--- a/solution.py
+++ b/solution.py
@@ -32,7 +32,9 @@
 
 
 def norm_rows(stream, gain):
-    whole = lax.all_gather(stream, "tp", axis=1, tiled=True)
+    size = lax.axis_size("tp")
+    repeats = [size if d == 1 else 1 for d in range(stream.ndim)]
+    whole = lax.all_to_all(jnp.tile(stream, repeats), "tp", split_axis=1, concat_axis=1, tiled=True)
     values = whole.astype(jnp.float32)
     scale = lax.rsqrt(jnp.mean(values * values, axis=1, keepdims=True) + epsilon)
     return (values * scale * gain).astype(jnp.bfloat16)

time: 432 us -> 409 us (0.947)
  waiting for transfers between devices: 328 us -> 267 us
  local copies, waits for them, and re-layouts: 6.23 us -> 26.7 us
  starting transfers between devices: 23 us -> 34.8 us
    all_gather x3, waiting for transfers between devices: 157 us -> 0.01 us  [sent_together(): lax.all_gather(both, axis, axis=dim, tiled=True)]
    all_to_all x0 -> x3, waiting for transfers between devices: none -> 112 us  [norm_rows(): lax.all_to_all(jnp.tile(stream, repeats), 'tp', split_axis=1, concat_axis...]
    all_gather x3 -> x0, waiting for transfers between devices: 63.2 us -> none  [norm_rows(): whole = lax.all_gather(stream, 'tp', axis=1, tiled=True)]
    all_to_all x3, waiting for transfers between devices: 0.01 us -> 51.2 us  [copy_for_each(): return lax.all_to_all(copies, axis, split_axis=0, concat_axis=0, tiled=True)]
    all_to_all x0 -> x3, starting transfers between devices: none -> 12.3 us  [norm_rows(): lax.all_to_all(jnp.tile(stream, repeats), 'tp', split_axis=1, concat_axis...]
    all_to_all x0 -> x3, local copies, waits for them, and re-layouts: none -> 9.56 us  [norm_rows(): lax.all_to_all(jnp.tile(stream, repeats), 'tp', split_axis=1, concat_axis...]
    another operation x0 -> x3, local copies, waits for them, and re-layouts: none -> 6.65 us  [norm_rows(): jnp.tile(stream, repeats)]
    convert_element_type x1 -> x3, other arithmetic: 0.79 us -> 7.37 us  [norm_rows(): return (values * scale * gain).astype(jnp.bfloat16)]
  transfers between devices with their start and end apart: 12 -> 12, of which waited for: 9 -> 8; matrix products, arithmetic and copies ran while one was open for 8% -> 13% of each run, Pallas kernels for 0% -> 0%
where the time goes in v1:
time: 409 us; the launch traced here: 408 us
  waiting for transfers between devices  267 us (65%)
  matrix products  46.9 us (11%)
  starting transfers between devices  34.8 us (9%)
  local copies, waits for them, and re-layouts  26.7 us (7%)
  other arithmetic  18.4 us (4%)
  between operations  13.7 us (3%)
    all_to_all x3, waiting for transfers between devices, norm_rows(): lax.all_to_all(jnp.tile(stream, repeats), 'tp', split_axis=1, concat_axis...  112 us
    reduce_scatter x3, waiting for transfers between devices, project_down(): lax.psum_scatter(partial_sum.astype(jnp.bfloat16), 'tp', scatter_dimensio...  104 us
    all_to_all x3, waiting for transfers between devices, copy_for_each(): return lax.all_to_all(copies, axis, split_axis=0, concat_axis=0, tiled=True)  51.2 us
    dot_general x3, matrix products, project_down(): jnp.dot(hidden, gathered_copies(weight, 'fs', 1), preferred_element_type=...  28.1 us
    all_to_all x3, starting transfers between devices, copy_for_each(): return lax.all_to_all(copies, axis, split_axis=0, concat_axis=0, tiled=True)  22 us
    dot_general x4, matrix products, add_rows(): return jnp.dot(gathered, piece, preferred_element_type=jnp.float32)  18.7 us
    all_to_all x3, starting transfers between devices, norm_rows(): lax.all_to_all(jnp.tile(stream, repeats), 'tp', split_axis=1, concat_axis...  12.3 us
    all_to_all x3, local copies, waits for them, and re-layouts, norm_rows(): lax.all_to_all(jnp.tile(stream, repeats), 'tp', split_axis=1, concat_axis...  9.56 us
  transfers between devices with their start and end apart: 12, of which 8 were waited for; matrix products, arithmetic and copies ran while one was open for 13% of the time, Pallas kernels for 0%

profile of v1, /device:TPU:0, one launch (start us, length us, event | category | flops | bytes accessed | tf_op | source)
XLA Modules:
  0.0 407.8 jit_solution(2424159184898974945)
XLA Ops:
  8.3 2.9 tile.6
  11.2 4.7 %all-to-all-start = ((bf16[768,8,256]{2,0,1:T(8,128)(2,1)}), bf16[768,8,256]{2,0,1:T(8,128)(2,1)S(1)}, u32[]{:S(2)}, u32[]{:S(2)}) async-start(bf16[768,8,256]{2,0,1:T(8,128)(2,1)} %tile.6), calls=%async_computation | async-start | bytes 6291456 | tf_op jit(solution)/shard_map/all_to_all | solution.py:37
  16.1 38.2 %all-to-all-done = bf16[768,8,256]{2,0,1:T(8,128)(2,1)S(1)} async-done(((bf16[768,8,256]{2,0,1:T(8,128)(2,1)}), bf16[768,8,256]{2,0,1:T(8,128)(2,1)S(1)}, u32[]{:S(2)}, u32[]{:S(2)}) %all-to-all-start) | async-done | bytes 3145760 | tf_op jit(solution)/shard_map/all_to_all | solution.py:37
  56.9 7.9 %all-to-all-start.1 = ((bf16[16,640,128]{1,2,0:T(8,128)(2,1)}), bf16[16,640,128]{1,2,0:T(8,128)(2,1)}, u32[]{:S(2)}, u32[]{:S(2)}) async-start(bf16[16,640,128]{1,2,0:T(8,128)(2,1)} %broadcast_in_dim.6), calls=%async_computation.1 | async-start | bytes 5242880 | tf_op jit(solution)/shard_map/all_to_all | solution.py:20
  64.9 3.2 copy.22
  71.3 6.8 %fusion.12 = f32[768,640]{1,0:T(8,128)} fusion(bf16[768,2048]{0,1:T(8,128)(2,1)} %fusion.5, bf16[2048,1280]{1,0:T(8,128)(2,1)} %all-gather.4.cloned.1.call-done), kind=kOutput, calls=%fused_computation.21 | convolution fusion | flops 2013265920 | bytes 7733248 | tf_op jit(solution)/shard_map/dot_general | solution.py:44
  78.1 25.7 %all-to-all-done.1 = bf16[16,640,128]{1,2,0:T(8,128)(2,1)} async-done(((bf16[16,640,128]{1,2,0:T(8,128)(2,1)}), bf16[16,640,128]{1,2,0:T(8,128)(2,1)}, u32[]{:S(2)}, u32[]{:S(2)}) %all-to-all-start.1) | async-done | bytes 2621472 | tf_op jit(solution)/shard_map/all_to_all | solution.py:20
  103.7 10.9 %convolution_convert_fusion.1 = bf16[768,2048]{1,0:T(8,128)(2,1)} fusion(bf16[640,2048]{0,1:T(8,128)(2,1)} %bitcast.3, f32[768,640]{1,0:T(8,128)} %fusion.12, bf16[768,2048]{0,1:T(8,128)(2,1)S(1)} %copy-done.6, bf16[2048,1280]{1,0:T(8,128)(2,1)} %all-gather.4.cloned.1.call-done), kind=kOutput, calls=%fused_computation.13 | convolution fusion | flops 4031053824 | bytes 13500416 | tf_op jit(solution)/shard_map/dot_general | solution.py:63
  114.7 36.3 %reduce-scatter.4.cloned.1.call-done = bf16[768,256]{1,0:T(8,128)(2,1)} async-done(((bf16[768,2048]{1,0:T(8,128)(2,1)}), bf16[768,256]{1,0:T(8,128)(2,1)}) %reduce-scatter.4.cloned.1.call-update) | async-done | bytes 393232 | tf_op jit(solution)/shard_map/reduce_scatter | solution.py:66
  153.9 3.8 all-to-all-start.2
  160.7 35.3 %all-to-all-done.2 = bf16[768,8,256]{2,0,1:T(8,128)(2,1)S(1)} async-done(((bf16[768,8,256]{2,0,1:T(8,128)(2,1)}), bf16[768,8,256]{2,0,1:T(8,128)(2,1)S(1)}, u32[]{:S(2)}, u32[]{:S(2)}) %all-to-all-start.2) | async-done | bytes 3145760 | tf_op jit(solution)/shard_map/all_to_all | solution.py:37
  197.8 7.1 %all-to-all-start.3 = ((bf16[16,128,128]{1,2,0:T(8,128)(2,1)}), bf16[16,128,128]{1,2,0:T(8,128)(2,1)}, u32[]{:S(2)}, u32[]{:S(2)}) async-start(bf16[16,128,128]{1,2,0:T(8,128)(2,1)} %broadcast_in_dim.7), calls=%async_computation.4 | async-start | bytes 1048576 | tf_op jit(solution)/shard_map/all_to_all | solution.py:20
  205.1 3.2 copy.24
  211.4 3.1 fusion.24
  217.5 6.4 %convolution_convert_fusion.2 = bf16[768,2048]{1,0:T(8,128)(2,1)} fusion(bf16[128,2048]{0,1:T(8,128)(2,1)} %bitcast.11, f32[768,128]{1,0:T(8,128)} %bitcast.50, bf16[768,2048]{0,1:T(8,128)(2,1)S(1)} %copy-done, bf16[2048,384]{1,0:T(8,128)(2,1)} %all-gather.6.cloned.1.call-done), kind=kOutput, calls=%fused_computation.14 | convolution fusion | flops 807075840 | bytes 7733248 | tf_op jit(solution)/shard_map/dot_general | solution.py:63
  225.7 34.0 %reduce-scatter.6.cloned.1.call-done = bf16[768,256]{1,0:T(8,128)(2,1)} async-done(((bf16[768,2048]{1,0:T(8,128)(2,1)}), bf16[768,256]{1,0:T(8,128)(2,1)}) %reduce-scatter.6.cloned.1.call-update) | async-done | bytes 393232 | tf_op jit(solution)/shard_map/reduce_scatter | solution.py:66
  263.4 3.8 all-to-all-start.4
  267.4 38.2 %all-to-all-done.4 = bf16[768,8,256]{2,0,1:T(8,128)(2,1)S(1)} async-done(((bf16[768,8,256]{2,0,1:T(8,128)(2,1)}), bf16[768,8,256]{2,0,1:T(8,128)(2,1)S(1)}, u32[]{:S(2)}, u32[]{:S(2)}) %all-to-all-start.4) | async-done | bytes 3145760 | tf_op jit(solution)/shard_map/all_to_all | solution.py:37
  308.1 7.0 %all-to-all-start.5 = ((bf16[16,640,128]{1,2,0:T(8,128)(2,1)}), bf16[16,640,128]{1,2,0:T(8,128)(2,1)}, u32[]{:S(2)}, u32[]{:S(2)}) async-start(bf16[16,640,128]{1,2,0:T(8,128)(2,1)} %broadcast_in_dim.8), calls=%async_computation.7 | async-start | bytes 5242880 | tf_op jit(solution)/shard_map/all_to_all | solution.py:20
  315.4 3.2 copy.26
  321.8 6.8 %fusion.8 = f32[768,640]{1,0:T(8,128)} fusion(bf16[768,2048]{0,1:T(8,128)(2,1)} %fusion.1, bf16[2048,1280]{1,0:T(8,128)(2,1)} %all-gather.8.cloned.1.call-done), kind=kOutput, calls=%fused_computation.17 | convolution fusion | flops 2013265920 | bytes 7733248 | tf_op jit(solution)/shard_map/dot_general | solution.py:44
  328.6 25.5 %all-to-all-done.5 = bf16[16,640,128]{1,2,0:T(8,128)(2,1)} async-done(((bf16[16,640,128]{1,2,0:T(8,128)(2,1)}), bf16[16,640,128]{1,2,0:T(8,128)(2,1)}, u32[]{:S(2)}, u32[]{:S(2)}) %all-to-all-start.5) | async-done | bytes 2621472 | tf_op jit(solution)/shard_map/all_to_all | solution.py:20
  354.0 10.9 %convolution_convert_fusion = bf16[768,2048]{1,0:T(8,128)(2,1)} fusion(bf16[640,2048]{0,1:T(8,128)(2,1)} %bitcast.14, f32[768,640]{1,0:T(8,128)} %fusion.8, bf16[768,2048]{0,1:T(8,128)(2,1)S(1)} %copy-done.7, bf16[2048,1280]{1,0:T(8,128)(2,1)} %all-gather.8.cloned.1.call-done), kind=kOutput, calls=%fused_computation.12 | convolution fusion | flops 4031053824 | bytes 13500416 | tf_op jit(solution)/shard_map/dot_general | solution.py:63
  365.0 34.1 %reduce-scatter.8.cloned.1.call-done = bf16[768,256]{1,0:T(8,128)(2,1)} async-done(((bf16[768,2048]{1,0:T(8,128)(2,1)}), bf16[768,256]{1,0:T(8,128)(2,1)}) %reduce-scatter.8.cloned.1.call-update) | async-done | bytes 393232 | tf_op jit(solution)/shard_map/reduce_scatter | solution.py:66
  (76 shorter events, 35.3 us)
Async XLA Ops:
  6.5 64.8 %all-gather.4.cloned.1.call-start = ((), (), s32[]{:S(2)}) async-start(), calls=%async_computation.9 | async-start | bytes 5570560 | tf_op jit(solution)/shard_map/all_gather | solution.py:15
  11.2 4.7 %copy-start.11 = (bf16[640,128]{1,0:T(8,128)(2,1)S(1)}, bf16[640,128]{1,0:T(8,128)(2,1)}, u32[]{:S(2)}) copy-start(bf16[640,128]{1,0:T(8,128)(2,1)} %param.19) | copy-start | bytes 491524
  11.2 43.1 %all-to-all-start = ((bf16[768,8,256]{2,0,1:T(8,128)(2,1)}), bf16[768,8,256]{2,0,1:T(8,128)(2,1)S(1)}, u32[]{:S(2)}, u32[]{:S(2)}) async-start(bf16[768,8,256]{2,0,1:T(8,128)(2,1)} %tile.6), calls=%async_computation | async-start | bytes 6291456 | tf_op jit(solution)/shard_map/all_to_all | solution.py:37
  54.3 2.6 copy-start.2
  56.9 46.8 %all-to-all-start.1 = ((bf16[16,640,128]{1,2,0:T(8,128)(2,1)}), bf16[16,640,128]{1,2,0:T(8,128)(2,1)}, u32[]{:S(2)}, u32[]{:S(2)}) async-start(bf16[16,640,128]{1,2,0:T(8,128)(2,1)} %broadcast_in_dim.6), calls=%async_computation.1 | async-start | bytes 5242880 | tf_op jit(solution)/shard_map/all_to_all | solution.py:20
  64.8 86.1 %reduce-scatter.4.cloned.1.call-start = ((), (), s32[]{:S(2)}) async-start(), calls=%async_computation.10 | async-start | bytes 3538944 | tf_op jit(solution)/shard_map/reduce_scatter | solution.py:66
  71.3 32.5 %copy-start.6 = (bf16[768,2048]{0,1:T(8,128)(2,1)S(1)}, bf16[768,2048]{0,1:T(8,128)(2,1)}, u32[]{:S(2)}) copy-start(bf16[768,2048]{0,1:T(8,128)(2,1)} %fusion.5) | copy-start | bytes 9437188
  114.6 36.3 %copy-start.8 = (bf16[2,384,256]{2,1,0:T(8,128)(2,1)S(1)}, bf16[2,384,256]{2,1,0:T(8,128)(2,1)}, u32[]{:S(2)}) copy-start(bf16[2,384,256]{2,1,0:T(8,128)(2,1)} %param.15) | copy-start | bytes 1179652
  153.9 6.8 %copy-start.16 = (f32[3,128]{1,0:T(4,128)S(1)}, f32[3,128]{1,0:T(4,128)}, u32[]{:S(2)}) copy-start(f32[3,128]{1,0:T(4,128)} %param.24) | copy-start | bytes 4612
  153.9 42.1 %all-to-all-start.2 = ((bf16[768,8,256]{2,0,1:T(8,128)(2,1)}), bf16[768,8,256]{2,0,1:T(8,128)(2,1)S(1)}, u32[]{:S(2)}, u32[]{:S(2)}) async-start(bf16[768,8,256]{2,0,1:T(8,128)(2,1)} %tile.7), calls=%async_computation.3 | async-start | bytes 6291456 | tf_op jit(solution)/shard_map/all_to_all | solution.py:37
  157.7 53.8 %all-gather.6.cloned.1.call-start = ((), (), s32[]{:S(2)}) async-start(), calls=%async_computation.11 | async-start | bytes 1671168 | tf_op jit(solution)/shard_map/all_gather | solution.py:15
  196.0 8.9 %copy-start.1 = (bf16[768,8,256]{2,0,1:T(8,128)(2,1)}, bf16[768,8,256]{2,0,1:T(8,128)(2,1)S(1)}, u32[]{:S(2)}) copy-start(bf16[768,8,256]{2,0,1:T(8,128)(2,1)S(1)} %all-to-all-done.2) | copy-start | bytes 9437188
  197.8 19.7 %all-to-all-start.3 = ((bf16[16,128,128]{1,2,0:T(8,128)(2,1)}), bf16[16,128,128]{1,2,0:T(8,128)(2,1)}, u32[]{:S(2)}, u32[]{:S(2)}) async-start(bf16[16,128,128]{1,2,0:T(8,128)(2,1)} %broadcast_in_dim.7), calls=%async_computation.4 | async-start | bytes 1048576 | tf_op jit(solution)/shard_map/all_to_all | solution.py:20
  204.9 54.8 %reduce-scatter.6.cloned.1.call-start = ((), (), s32[]{:S(2)}) async-start(), calls=%async_computation.12 | async-start | bytes 3538944 | tf_op jit(solution)/shard_map/reduce_scatter | solution.py:66
  211.4 3.2 copy-start
  223.9 1.0 copy-start.10
  223.9 97.8 %all-gather.8.cloned.1.call-start = ((), (), s32[]{:S(2)}) async-start(), calls=%async_computation.13 | async-start | bytes 5570560 | tf_op jit(solution)/shard_map/all_gather | solution.py:15
  263.4 3.8 copy-start.12
  263.4 42.1 %all-to-all-start.4 = ((bf16[768,8,256]{2,0,1:T(8,128)(2,1)}), bf16[768,8,256]{2,0,1:T(8,128)(2,1)S(1)}, u32[]{:S(2)}, u32[]{:S(2)}) async-start(bf16[768,8,256]{2,0,1:T(8,128)(2,1)} %tile.8), calls=%async_computation.6 | async-start | bytes 6291456 | tf_op jit(solution)/shard_map/all_to_all | solution.py:37
  305.6 2.6 copy-start.3
  308.1 45.9 %all-to-all-start.5 = ((bf16[16,640,128]{1,2,0:T(8,128)(2,1)}), bf16[16,640,128]{1,2,0:T(8,128)(2,1)}, u32[]{:S(2)}, u32[]{:S(2)}) async-start(bf16[16,640,128]{1,2,0:T(8,128)(2,1)} %broadcast_in_dim.8), calls=%async_computation.7 | async-start | bytes 5242880 | tf_op jit(solution)/shard_map/all_to_all | solution.py:20
  315.1 84.0 %reduce-scatter.8.cloned.1.call-start = ((), (), s32[]{:S(2)}) async-start(), calls=%async_computation.14 | async-start | bytes 3538944 | tf_op jit(solution)/shard_map/reduce_scatter | solution.py:66
  321.8 32.3 %copy-start.7 = (bf16[768,2048]{0,1:T(8,128)(2,1)S(1)}, bf16[768,2048]{0,1:T(8,128)(2,1)}, u32[]{:S(2)}) copy-start(bf16[768,2048]{0,1:T(8,128)(2,1)} %fusion.1) | copy-start | bytes 9437188
  364.9 34.2 %copy-start.5 = (bf16[768,256]{1,0:T(8,128)(2,1)S(1)}, bf16[768,256]{1,0:T(8,128)(2,1)}, u32[]{:S(2)}) copy-start(bf16[768,256]{1,0:T(8,128)(2,1)} %copy-done.4) | copy-start | bytes 1179652
  (5 other events, 3.8 us)
Sparse Core Ops, SparseCore 0:
  9.5 58.8 all-gather.3
  114.8 36.1 reduce-scatter.3
  160.6 45.5 all-gather.5
  224.1 35.5 reduce-scatter.5
  261.7 55.1 all-gather.7
  365.1 33.9 reduce-scatter.7
